TPU v7x, 32 devices: a whole 2x2x4 slice. The times are simulated.
32 devices in a mesh: sp: 4 (over x, core), dp: 8 (over z, y).
Axes of the slice: x: 2, y: 2, z: 4, core: 2. Of those that a mesh axis runs over, the one named last changes fastest.
Arguments:
- queries: bfloat16 [16, 8, 576, 128], P('dp', None, 'sp'), may hold values from -6 to 6
- keys: bfloat16 [16, 8, 576, 128], P('dp', None, 'sp'), may hold values from -6 to 6
- values: bfloat16 [16, 8, 576, 128], P('dp', None, 'sp'), may hold values from -6 to 6
- in_gate: bfloat16 [16, 8, 576], P('dp', None, 'sp'), may hold values from -5 to 240
- forget_gate: bfloat16 [16, 8, 576], P('dp', None, 'sp'), may hold values from 1 to 20
- out_gate: bfloat16 [16, 8, 576, 128], P('dp', None, 'sp'), may hold values from -6 to 6
- norm_gain: float32 [8, 128], replicated, may hold values from 0.1 to 1.9
- out_weight: bfloat16 [1024, 2048], P(None, 'dp'), may hold values from -0.1875 to 0.1875
Outputs:
- mixed: bfloat16 [16, 576, 2048], P('dp', 'sp')
All inputs are finite; a program needn't handle non-finite values.
Results may differ from a plain program's by a relative error of at most 0.0057.
Values may be sent and summed in bfloat16 or wider, within the bound.
A program may use at most 64 MiB of HBM per device.

v0:
```python
import jax
import jax.numpy as jnp
from jax import lax
from jax.sharding import PartitionSpec as P

BLK = 64
highest = lax.Precision.HIGHEST
norm_eps = 1e-05


def run_cells(parts):
    query_in, key_in, value_in, input_in, forget_in = parts
    item_count = query_in.shape[1]
    seq_len = query_in.shape[2]
    head_size = query_in.shape[3]
    blocks = seq_len // BLK
    key_scale = head_size ** (-0.5)
    query_b = query_in.reshape(item_count, blocks, BLK, head_size)
    key_b = key_in.reshape(item_count, blocks, BLK, head_size)
    value_b = value_in.reshape(item_count, blocks, BLK, head_size)
    input_b = input_in.astype(jnp.float32).reshape(item_count, blocks, BLK)
    logf_b = jax.nn.log_sigmoid(forget_in.astype(jnp.float32)).reshape(item_count, blocks, BLK)
    cumulative = jnp.cumsum(logf_b, axis=-1)
    block_end = cumulative[..., -1]
    growth = block_end[..., None] - cumulative + input_b
    growth_max = jnp.max(growth, axis=-1)
    w_key = jnp.exp(growth - growth_max[..., None]) * key_scale
    key_f = key_b.astype(jnp.float32)
    value_f = value_b.astype(jnp.float32)
    weighted = w_key[..., None] * key_f
    fresh_memory = jnp.einsum("ncsd,ncse->ncde", weighted, value_f, precision=highest)
    fresh_norm = jnp.sum(weighted, axis=2)

    def advance(state_in, inputs):
        memory, normalizer, stabilizer = state_in
        end_now, top_now, memory_add, norm_add = inputs
        stab_new = jnp.maximum(end_now + stabilizer, top_now)
        decay_old = jnp.exp(end_now + stabilizer - stab_new)
        decay_add = jnp.exp(top_now - stab_new)
        memory_new = decay_old[:, None, None] * memory + decay_add[:, None, None] * memory_add
        norm_new = decay_old[:, None] * normalizer + decay_add[:, None] * norm_add
        return ((memory_new, norm_new, stab_new), (memory, normalizer, stabilizer))

    start = (
        jnp.zeros((item_count, head_size, head_size), jnp.float32),
        jnp.zeros((item_count, head_size), jnp.float32),
        jnp.zeros((item_count,), jnp.float32),
    )
    series = (
        jnp.swapaxes(block_end, 0, 1),
        jnp.swapaxes(growth_max, 0, 1),
        jnp.swapaxes(fresh_memory, 0, 1),
        jnp.swapaxes(fresh_norm, 0, 1),
    )
    _, (memory_prev, norm_prev, stab_prev) = lax.scan(advance, start, series)
    memory_prev = jnp.swapaxes(memory_prev, 0, 1)
    norm_prev = jnp.swapaxes(norm_prev, 0, 1)
    stab_prev = jnp.swapaxes(stab_prev, 0, 1)
    causal_mask = jnp.tril(jnp.ones((BLK, BLK), dtype=bool))
    log_weights = cumulative[..., :, None] - cumulative[..., None, :] + input_b[..., None, :]
    log_weights = jnp.where(causal_mask, log_weights, -jnp.inf)
    carried_log = cumulative + stab_prev[..., None]
    row_max = jnp.maximum(jnp.max(log_weights, axis=-1), carried_log)
    w_intra = jnp.exp(log_weights - row_max[..., None])
    w_inter = jnp.exp(carried_log - row_max)
    scores = jnp.einsum("ncpd,ncqd->ncpq", query_b, key_b, preferred_element_type=jnp.float32) * (
        key_scale * w_intra
    )
    query_f = query_b.astype(jnp.float32)
    numerator = w_inter[..., None] * jnp.einsum(
        "ncpd,ncde->ncpe", query_f, memory_prev, precision=highest
    )
    numerator = numerator + jnp.einsum("ncpq,ncqe->ncpe", scores, value_f, precision=highest)
    denominator = w_inter * jnp.einsum(
        "ncpd,ncd->ncp", query_f, norm_prev, precision=highest
    ) + jnp.sum(scores, axis=-1)
    cell_out = numerator / jnp.maximum(jnp.abs(denominator), 1.0)[..., None]
    return cell_out.reshape(1, item_count, seq_len, head_size).astype(jnp.bfloat16)


def body(queries, keys, values, in_gate, forget_gate, out_gate, norm_gain, out_weight):
    rank_count = lax.axis_size("sp")
    group_seqs, head_count, span_len, head_size = queries.shape

    def by_rank(array):
        return array.reshape((rank_count, -1) + array.shape[2:])

    cell_out = run_cells(
        (
            lax.all_to_all(by_rank(queries), "sp", split_axis=0, concat_axis=2, tiled=True),
            lax.all_to_all(by_rank(keys), "sp", split_axis=0, concat_axis=2, tiled=True),
            lax.all_to_all(by_rank(values), "sp", split_axis=0, concat_axis=2, tiled=True),
            lax.all_to_all(by_rank(in_gate), "sp", split_axis=0, concat_axis=2, tiled=True),
            lax.all_to_all(by_rank(forget_gate), "sp", split_axis=0, concat_axis=2, tiled=True),
        )
    )
    returned = lax.all_to_all(cell_out, "sp", split_axis=2, concat_axis=0, tiled=True)
    returned = returned.reshape(group_seqs, head_count, span_len, head_size).astype(jnp.float32)
    mean_val = jnp.mean(returned, axis=-1, keepdims=True)
    centered = returned - mean_val
    variance = jnp.mean(centered * centered, axis=-1, keepdims=True)
    normed = centered * lax.rsqrt(variance + norm_eps) * norm_gain[None, :, None, :]
    hidden = (normed * jax.nn.sigmoid(out_gate.astype(jnp.float32))).astype(jnp.bfloat16)
    hidden = jnp.swapaxes(hidden, 1, 2).reshape(group_seqs * span_len, head_count * head_size)
    result = jnp.dot(
        hidden,
        lax.all_gather(out_weight, "dp", axis=1, tiled=True),
        preferred_element_type=jnp.float32,
    )
    return result.astype(jnp.bfloat16).reshape(group_seqs, span_len, -1)


def solution(mesh):
    return jax.shard_map(
        body,
        mesh=mesh,
        in_specs=(
            P("dp", None, "sp", None),
            P("dp", None, "sp", None),
            P("dp", None, "sp", None),
            P("dp", None, "sp"),
            P("dp", None, "sp"),
            P("dp", None, "sp", None),
            P(),
            P(None, "dp"),
        ),
        out_specs=P("dp", "sp", None),
        check_vma=False,
    )
```

profile of v0, /device:TPU:0, one launch (start us, length us, event | category | flops | bytes accessed | tf_op | source)
XLA Modules:
  0.0 103.2 jit_solution(3290982956562113304)
XLA Ops:
  6.5 1.3 %reshape.170 = bf16[4,4,144]{2,1,0:T(4,128)(2,1)} reshape(bf16[2,8,144]{2,1,0:T(8,128)(2,1)} %param.14) | data formatting | bytes 9216 | tf_op jit(solution)/shard_map/reshape | solution.py:86
  7.8 4.2 %all-to-all-start = ((bf16[4,4,144]{2,1,0:T(4,128)(2,1)}), bf16[4,4,144]{2,1,0:T(4,128)(2,1)S(1)}, u32[]{:S(2)}, u32[]{:S(2)}) async-start(bf16[4,4,144]{2,1,0:T(4,128)(2,1)} %reshape.170), calls=%async_computation | async-start | bytes 16384 | tf_op jit(solution)/shard_map/all_to_all | solution.py:94
  12.1 0.7 all-gather.2.cloned.1.call-update
  12.9 1.3 %reshape.171 = bf16[4,4,144]{2,1,0:T(4,128)(2,1)} reshape(bf16[2,8,144]{2,1,0:T(8,128)(2,1)} %param.13) | data formatting | bytes 9216 | tf_op jit(solution)/shard_map/reshape | solution.py:86
  14.2 1.7 %all-to-all-done = bf16[4,4,144]{2,1,0:T(4,128)(2,1)S(1)} async-done(((bf16[4,4,144]{2,1,0:T(4,128)(2,1)}), bf16[4,4,144]{2,1,0:T(4,128)(2,1)S(1)}, u32[]{:S(2)}, u32[]{:S(2)}) %all-to-all-start) | async-done | bytes 4640 | tf_op jit(solution)/shard_map/all_to_all | solution.py:94
  15.9 3.2 %all-to-all-start.1 = ((bf16[4,4,144]{2,1,0:T(4,128)(2,1)}), bf16[4,4,144]{2,1,0:T(4,128)(2,1)S(1)}, u32[]{:S(2)}, u32[]{:S(2)}) async-start(bf16[4,4,144]{2,1,0:T(4,128)(2,1)} %reshape.171), calls=%async_computation.1 | async-start | bytes 16384 | tf_op jit(solution)/shard_map/all_to_all | solution.py:93
  19.2 3.8 %all-to-all-done.1 = bf16[4,4,144]{2,1,0:T(4,128)(2,1)S(1)} async-done(((bf16[4,4,144]{2,1,0:T(4,128)(2,1)}), bf16[4,4,144]{2,1,0:T(4,128)(2,1)S(1)}, u32[]{:S(2)}, u32[]{:S(2)}) %all-to-all-start.1) | async-done | bytes 4640 | tf_op jit(solution)/shard_map/all_to_all | solution.py:93
  22.9 3.5 %all-to-all-start.2 = ((bf16[4,4,144,128]{3,2,1,0:T(8,128)(2,1)}), bf16[4,4,144,128]{3,2,1,0:T(8,128)(2,1)S(1)}, u32[]{:S(2)}, u32[]{:S(2)}) async-start(bf16[4,4,144,128]{3,2,1,0:T(8,128)(2,1)} %bitcast.130), calls=%async_computation.2 | async-start | bytes 1179648 | tf_op jit(solution)/shard_map/all_to_all | solution.py:91
  26.5 0.1 neg.37
  26.5 0.1 reshape.180
  26.7 0.9 reduce_window_sum.11
  27.6 0.2 slice_reduce_fusion
  27.7 8.2 %all-to-all-done.2 = bf16[4,4,144,128]{3,2,1,0:T(8,128)(2,1)S(1)} async-done(((bf16[4,4,144,128]{3,2,1,0:T(8,128)(2,1)}), bf16[4,4,144,128]{3,2,1,0:T(8,128)(2,1)S(1)}, u32[]{:S(2)}, u32[]{:S(2)}) %all-to-all-start.2) | async-done | bytes 589856 | tf_op jit(solution)/shard_map/all_to_all | solution.py:91
  35.9 3.5 %all-to-all-start.3 = ((bf16[4,4,144,128]{3,2,1,0:T(8,128)(2,1)}), bf16[4,4,144,128]{3,2,1,0:T(8,128)(2,1)S(1)}, u32[]{:S(2)}, u32[]{:S(2)}) async-start(bf16[4,4,144,128]{3,2,1,0:T(8,128)(2,1)} %bitcast.10), calls=%async_computation.3 | async-start | bytes 1179648 | tf_op jit(solution)/shard_map/all_to_all | solution.py:92
  39.4 0.2 fusion.29
  39.6 0.1 copy.72
  39.7 0.1 copy.71
  39.7 0.8 fusion.16
  40.5 0.1 exponential_multiply_fusion
  40.7 8.2 %all-to-all-done.3 = bf16[4,4,144,128]{3,2,1,0:T(8,128)(2,1)S(1)} async-done(((bf16[4,4,144,128]{3,2,1,0:T(8,128)(2,1)}), bf16[4,4,144,128]{3,2,1,0:T(8,128)(2,1)S(1)}, u32[]{:S(2)}, u32[]{:S(2)}) %all-to-all-start.3) | async-done | bytes 589856 | tf_op jit(solution)/shard_map/all_to_all | solution.py:92
  48.9 4.2 %all-to-all-start.4 = ((bf16[4,4,144,128]{3,2,1,0:T(8,128)(2,1)}), bf16[4,4,144,128]{3,2,1,0:T(8,128)(2,1)}, u32[]{:S(2)}, u32[]{:S(2)}) async-start(bf16[4,4,144,128]{3,2,1,0:T(8,128)(2,1)} %bitcast.18), calls=%async_computation.4 | async-start | bytes 1179648 | tf_op jit(solution)/shard_map/all_to_all | solution.py:90
  53.1 0.4 fusion.17
  53.5 2.4 %convolution_bitcast_fusion = f32[9,4,128,128]{3,2,0,1:T(8,128)S(1)} fusion(bf16[4,9,64,128]{3,2,1,0:T(8,128)(2,1)S(1)} %bitcast.123, bf16[4,9,64,128]{3,2,1,0:T(8,128)(2,1)S(1)} %bitcast.120, f32[4,9,64]{2,1,0:T(8,128)S(1)} %exponential_multiply_fusion), kind=kOutput, calls=%fused_computation.19 | convolution fusion | flops 453574656 | bytes 3548160 | tf_op jit(solution)/shard_map/ncsd,ncse->ncde/dot_general | solution.py:31
  55.9 9.3 %while.21 = (s32[]{:T(128)}, f32[4,128,128]{2,1,0:T(8,128)S(1)}, f32[4,128]{1,0:T(4,128)S(1)}, f32[4]{0:T(128)S(1)}, f32[9,4,128,128]{3,2,1,0:T(8,128)}, /*index...) while((s32[]{:T(128)}, f32[4,128,128]{2,1,0:T(8,128)S(1)}, ...), condition=%wide.region_4.5_spmd.clone, body=%wide.region_3.4_spmd.clone.sunk | while | flops 330263 | bytes 1325971 | solution.py:55
  56.0 0.7 bitcast_dynamic-update-slice_fusion.4
  56.7 0.1 fusion.42
  56.8 0.1 multiply_add_fusion.2
  57.0 0.7 bitcast_dynamic-update-slice_fusion.4
  57.7 0.1 fusion.42
  58.0 0.7 bitcast_dynamic-update-slice_fusion.4
  58.7 0.1 fusion.42
  58.9 0.1 multiply_add_fusion.2
  59.0 0.7 bitcast_dynamic-update-slice_fusion.4
  59.8 0.1 fusion.42
  59.9 0.1 multiply_add_fusion.2
  60.1 0.7 bitcast_dynamic-update-slice_fusion.4
  60.8 0.1 fusion.42
  61.0 0.1 multiply_add_fusion.2
  61.1 0.7 bitcast_dynamic-update-slice_fusion.4
  61.9 0.1 fusion.42
  62.2 0.7 bitcast_dynamic-update-slice_fusion.4
  62.9 0.1 fusion.42
  63.2 0.7 bitcast_dynamic-update-slice_fusion.4
  63.9 0.1 fusion.42
  64.2 0.7 bitcast_dynamic-update-slice_fusion.4
  65.0 0.1 fusion.42
  65.2 0.1 copy.75
  65.3 1.1 %copy.76 = bf16[1,4,4,144,128]{4,3,2,1,0:T(8,128)(2,1)S(1)} copy(bf16[1,4,4,144,128]{4,3,1,2,0:T(8,128)(2,1)} %bitcast.20) | data formatting | bytes 1179648 | tf_op jit(solution)/shard_map/all_to_all | solution.py:90
  66.5 1.0 fusion.27
  67.5 0.7 fusion.31
  68.3 0.1 fusion.26
  68.4 0.9 copy-done.2
  69.2 1.3 %fusion.11 = f32[4,9,64,128]{3,2,1,0:T(8,128)S(1)} fusion(bf16[4,9,64,128]{3,2,1,0:T(8,128)(2,1)S(1)} %bitcast.129, f32[4,9,64]{2,1,0:T(8,128)S(1)} %get-tuple-element.183, f32[9,4,128,128]{3,2,1,0:T(8,128)S(1)} %copy-done.2), kind=kOutput, calls=%fused_computation.21 | convolution fusion | flops 453279744 | bytes 4137984 | tf_op jit(solution)/shard_map/ncpd,ncde->ncpe/dot_general | solution.py:70
  70.6 1.3 %fusion.15 = bf16[4,9,64,128]{3,2,1,0:T(8,128)(2,1)S(1)} fusion(f32[4,9,64,128]{3,2,1,0:T(8,128)S(1)} %fusion.11, f32[4,9,64,64]{2,3,1,0:T(8,128)S(1)} %get-tuple-element.186, bf16[4,9,64,128]{3,2,1,0:T(8,128)(2,1)S(1)} %bitcast.124, f32[4,9,64]{2,1,0:T(8,128)S(1)} %get-tuple-element.182), kind=kOutput, calls=%fused_computation.25 | convolution fusion | flops 227377152 | bytes 2958336 | tf_op jit(solution)/shard_map/ncpq,ncqe->ncpe/dot_general | solution.py:73
  71.9 0.5 copy.79
  72.4 12.6 %all_to_all.72 = bf16[1,4,576,128]{3,1,0,2:T(4,128)(2,1)S(1)} all-to-all(bf16[1,4,576,128]{3,1,0,2:T(4,128)(2,1)S(1)} %copy.79), channel_id=1, replica_groups=mesh['sp'=4,'dp'=8] {'sp'}, dimensions={2} | all-to-all | bytes 1179648 | tf_op jit(solution)/shard_map/all_to_all | solution.py:97
  85.1 0.7 fusion.18
  85.8 0.2 copy.91
  86.0 1.4 %multiply_reduce_fusion = f32[4,4,144]{1,2,0:T(8,128)S(1)} fusion(bf16[1,4,4,144,128]{4,1,3,2,0:T(4,128)(2,1)S(1)} %bitcast.118, f32[4,4,144]{1,2,0:T(8,128)S(1)} %broadcast_multiply_fusion), kind=kLoop, calls=%fused_computation.28 | loop fusion | flops 1177344 | bytes 608256 | tf_op jit(solution)/shard_map/reduce_sum | solution.py:101
  87.5 0.2 copy.92
  87.8 0.8 fusion.22
  88.6 0.2 copy.84
  88.7 3.1 %all-gather.2.cloned.1.call-done = bf16[1024,2048]{1,0:T(8,128)(2,1)} async-done(((bf16[1024,256]{1,0:T(8,128)(2,1)}), bf16[1024,2048]{1,0:T(8,128)(2,1)}) %all-gather.2.cloned.1.call-update) | async-done | bytes 4194320 | tf_op jit(solution)/shard_map/all_gather | solution.py:107
  91.8 4.6 %convolution_convert_fusion = bf16[288,2048]{1,0:T(8,128)(2,1)} fusion(bf16[1024,2048]{1,0:T(8,128)(2,1)} %all-gather.2.cloned.1.call-done, bf16[36,8,8,128]{3,2,1,0:T(8,128)(2,1)S(1)} %bitcast.131), kind=kOutput, calls=%fused_computation.16 | convolution fusion | flops 1208549376 | bytes 5963776 | tf_op jit(solution)/shard_map/dot_general | solution.py:105
  (82 shorter events, 1.7 us)
Async XLA Ops:
  7.8 8.1 %all-to-all-start = ((bf16[4,4,144]{2,1,0:T(4,128)(2,1)}), bf16[4,4,144]{2,1,0:T(4,128)(2,1)S(1)}, u32[]{:S(2)}, u32[]{:S(2)}) async-start(bf16[4,4,144]{2,1,0:T(4,128)(2,1)} %reshape.170), calls=%async_computation | async-start | bytes 16384 | tf_op jit(solution)/shard_map/all_to_all | solution.py:94
  12.1 79.7 %all-gather.2.cloned.1.call-start = ((), (), s32[]{:S(2)}) async-start(), calls=%async_computation.6 | async-start | bytes 4718592 | tf_op jit(solution)/shard_map/all_gather | solution.py:107
  15.9 7.0 %all-to-all-start.1 = ((bf16[4,4,144]{2,1,0:T(4,128)(2,1)}), bf16[4,4,144]{2,1,0:T(4,128)(2,1)S(1)}, u32[]{:S(2)}, u32[]{:S(2)}) async-start(bf16[4,4,144]{2,1,0:T(4,128)(2,1)} %reshape.171), calls=%async_computation.1 | async-start | bytes 16384 | tf_op jit(solution)/shard_map/all_to_all | solution.py:93
  22.9 13.0 %all-to-all-start.2 = ((bf16[4,4,144,128]{3,2,1,0:T(8,128)(2,1)}), bf16[4,4,144,128]{3,2,1,0:T(8,128)(2,1)S(1)}, u32[]{:S(2)}, u32[]{:S(2)}) async-start(bf16[4,4,144,128]{3,2,1,0:T(8,128)(2,1)} %bitcast.130), calls=%async_computation.2 | async-start | bytes 1179648 | tf_op jit(solution)/shard_map/all_to_all | solution.py:91
  35.9 13.0 %all-to-all-start.3 = ((bf16[4,4,144,128]{3,2,1,0:T(8,128)(2,1)}), bf16[4,4,144,128]{3,2,1,0:T(8,128)(2,1)S(1)}, u32[]{:S(2)}, u32[]{:S(2)}) async-start(bf16[4,4,144,128]{3,2,1,0:T(8,128)(2,1)} %bitcast.10), calls=%async_computation.3 | async-start | bytes 1179648 | tf_op jit(solution)/shard_map/all_to_all | solution.py:92
  48.9 16.4 %all-to-all-start.4 = ((bf16[4,4,144,128]{3,2,1,0:T(8,128)(2,1)}), bf16[4,4,144,128]{3,2,1,0:T(8,128)(2,1)}, u32[]{:S(2)}, u32[]{:S(2)}) async-start(bf16[4,4,144,128]{3,2,1,0:T(8,128)(2,1)} %bitcast.18), calls=%async_computation.4 | async-start | bytes 1179648 | tf_op jit(solution)/shard_map/all_to_all | solution.py:90
  53.1 2.8 %copy-start = (bf16[1,4,4,144,128]{4,3,2,1,0:T(8,128)(2,1)}, bf16[1,4,4,144,128]{4,3,2,1,0:T(8,128)(2,1)S(1)}, u32[]{:S(2)}) copy-start(bf16[1,4,4,144,128]{4,3,2,1,0:T(8,128)(2,1)S(1)} %copy.70) | copy-start | bytes 1769476
  67.5 1.7 %copy-start.2 = (f32[9,4,128,128]{3,2,1,0:T(8,128)S(1)}, f32[9,4,128,128]{3,2,1,0:T(8,128)}, u32[]{:S(2)}) copy-start(f32[9,4,128,128]{3,2,1,0:T(8,128)} %get-tuple-element.65) | copy-start | bytes 7077892
  69.2 1.3 %copy-start.1 = (bf16[1,4,4,144,128]{4,3,2,1,0:T(8,128)(2,1)S(1)}, bf16[1,4,4,144,128]{4,3,2,1,0:T(8,128)(2,1)}, u32[]{:S(2)}) copy-start(bf16[1,4,4,144,128]{4,3,2,1,0:T(8,128)(2,1)} %copy-done) | copy-start | bytes 1769476
  85.8 1.9 %copy-start.3 = (bf16[2,8,144,128]{3,2,1,0:T(8,128)(2,1)S(1)}, bf16[2,8,144,128]{3,2,1,0:T(8,128)(2,1)}, u32[]{:S(2)}) copy-start(bf16[2,8,144,128]{3,2,1,0:T(8,128)(2,1)} %param.15) | copy-start | bytes 1769476
  85.8 1.9 %copy-start.4 = (f32[8,128]{1,0:T(8,128)S(1)}, f32[8,128]{1,0:T(8,128)}, u32[]{:S(2)}) copy-start(f32[8,128]{1,0:T(8,128)} %param.16) | copy-start | bytes 12292
Sparse Core Ops, SparseCore 0:
  14.9 76.8 all-gather.1
where the time goes:
time: 104 us; the launch traced here: 103 us
  waiting for transfers between devices  25.6 us (25%)
  starting transfers between devices  18.6 us (18%)
  other arithmetic  14.3 us (14%)
  between operations  13.7 us (13%)
  blocking collectives  12.6 us (12%)
  matrix products  11.4 us (11%)
  local copies, waits for them, and re-layouts  6.74 us (6%)
    all_to_all x1, blocking collectives, body(): lax.all_to_all(cell_out, 'sp', split_axis=2, concat_axis=0, tiled=True)  12.6 us
    all_to_all x1, waiting for transfers between devices, body(): lax.all_to_all(by_rank(keys), 'sp', split_axis=0, concat_axis=2, tiled=True)  8.19 us
    all_to_all x1, waiting for transfers between devices, body(): lax.all_to_all(by_rank(values), 'sp', split_axis=0, concat_axis=2, tiled=...  8.19 us
    dynamic_update_slice x18, other arithmetic, run_cells(): _, (memory_prev, norm_prev, stab_prev) = lax.scan(advance, start, series)  6.71 us
    dot_general x1, matrix products, body(): jnp.dot(hidden, lax.all_gather(out_weight, 'dp', axis=1, tiled=True), pre...  4.59 us
    all_to_all x1, starting transfers between devices, body(): lax.all_to_all(by_rank(forget_gate), 'sp', split_axis=0, concat_axis=2, t...  4.24 us
    all_to_all x1, starting transfers between devices, body(): lax.all_to_all(by_rank(queries), 'sp', split_axis=0, concat_axis=2, tiled...  4.15 us
    all_to_all x1, waiting for transfers between devices, body(): lax.all_to_all(by_rank(in_gate), 'sp', split_axis=0, concat_axis=2, tiled...  3.76 us
  transfers between devices with their start and end apart: 6, of which 5 were waited for; matrix products, arithmetic and copies ran while one was open for 25% of the time, Pallas kernels for 0%

commit v1 on v0

--- a/solution.py
+++ b/solution.py
@@ -6,6 +6,30 @@
 BLK = 64
 highest = lax.Precision.HIGHEST
 norm_eps = 1e-05
+
+
+def split_up(x, dim, size):
+    shape = x.shape
+    blocks = x.reshape(*shape[:dim], size, shape[dim] // size, *shape[dim + 1 :])
+    return jnp.moveaxis(blocks, dim, 0)
+
+
+def in_order(blocks, dim):
+    shape = list(blocks.shape[1:])
+    shape[dim] *= blocks.shape[0]
+    return jnp.moveaxis(blocks, 0, dim).reshape(shape)
+
+
+def sent_to_each(array, axis, split_dim, concat_dim):
+    size, index = (lax.axis_size(axis), lax.axis_index(axis))
+    parts = split_up(array, split_dim, size)
+    whole = parts
+    for step in range(1, size):
+        target, source = ((index + step) % size, (index - step) % size)
+        sent = lax.dynamic_index_in_dim(parts, target, 0)
+        other = lax.ppermute(sent, axis, [(i, (i + step) % size) for i in range(size)])
+        whole = lax.dynamic_update_slice_in_dim(whole, other, source, axis=0)
+    return in_order(whole, concat_dim)
 
 
 def run_cells(parts):
@@ -91,7 +115,7 @@
             lax.all_to_all(by_rank(keys), "sp", split_axis=0, concat_axis=2, tiled=True),
             lax.all_to_all(by_rank(values), "sp", split_axis=0, concat_axis=2, tiled=True),
             lax.all_to_all(by_rank(in_gate), "sp", split_axis=0, concat_axis=2, tiled=True),
-            lax.all_to_all(by_rank(forget_gate), "sp", split_axis=0, concat_axis=2, tiled=True),
+            sent_to_each(by_rank(forget_gate), "sp", 0, 2),
         )
     )
     returned = lax.all_to_all(cell_out, "sp", split_axis=2, concat_axis=0, tiled=True)

time: 104 us -> 108 us (1.038)
  waiting for transfers between devices: 25.6 us -> 29.5 us
    all_gather x1, waiting for transfers between devices: 3.06 us -> 9.7 us  [body(): lax.all_gather(out_weight, 'dp', axis=1, tiled=True)]
    ppermute x0 -> x3, starting transfers between devices: none -> 4.48 us  [sent_to_each(): lax.ppermute(sent, axis, [(i, (i + step) % size) for i in range(size)])]
    all_to_all x1 -> x0, starting transfers between devices: 4.24 us -> none  [body(): lax.all_to_all(by_rank(forget_gate), 'sp', split_axis=0, concat_axis=2, t...]
    all_to_all x1 -> x0, waiting for transfers between devices: 1.71 us -> none  [body(): lax.all_to_all(by_rank(forget_gate), 'sp', split_axis=0, concat_axis=2, t...]
    reshape x2 -> x1, local copies, waits for them, and re-layouts: 2.61 us -> 1.3 us  [by_rank(): return array.reshape((rank_count, -1) + array.shape[2:])]
    all_to_all x1, waiting for transfers between devices: 3.76 us -> 2.62 us  [body(): lax.all_to_all(by_rank(in_gate), 'sp', split_axis=0, concat_axis=2, tiled...]
  transfers between devices with their start and end apart: 6 -> 8, of which waited for: 5 -> 4; matrix products, arithmetic and copies ran while one was open for 25% -> 24% of each run, Pallas kernels for 0% -> 0%
where the time goes in v1:
time: 108 us; the launch traced here: 107 us
  waiting for transfers between devices  29.5 us (27%)
  starting transfers between devices  18.9 us (17%)
  other arithmetic  14.3 us (13%)
  between operations  13.8 us (13%)
  blocking collectives  12.6 us (12%)
  matrix products  11.4 us (11%)
  local copies, waits for them, and re-layouts  6.3 us (6%)
    all_to_all x1, blocking collectives, body(): lax.all_to_all(cell_out, 'sp', split_axis=2, concat_axis=0, tiled=True)  12.6 us
    all_gather x1, waiting for transfers between devices, body(): lax.all_gather(out_weight, 'dp', axis=1, tiled=True)  9.7 us
    all_to_all x1, waiting for transfers between devices, body(): lax.all_to_all(by_rank(values), 'sp', split_axis=0, concat_axis=2, tiled=...  8.28 us
    all_to_all x1, waiting for transfers between devices, body(): lax.all_to_all(by_rank(keys), 'sp', split_axis=0, concat_axis=2, tiled=True)  8.18 us
    dynamic_update_slice x18, other arithmetic, run_cells(): _, (memory_prev, norm_prev, stab_prev) = lax.scan(advance, start, series)  6.75 us
    dot_general x1, matrix products, body(): jnp.dot(hidden, lax.all_gather(out_weight, 'dp', axis=1, tiled=True), pre...  4.59 us
    ppermute x3, starting transfers between devices, sent_to_each(): lax.ppermute(sent, axis, [(i, (i + step) % size) for i in range(size)])  4.48 us
    all_to_all x1, starting transfers between devices, body(): lax.all_to_all(by_rank(queries), 'sp', split_axis=0, concat_axis=2, tiled...  4.15 us
  transfers between devices with their start and end apart: 8, of which 4 were waited for; matrix products, arithmetic and copies ran while one was open for 24% of the time, Pallas kernels for 0%

profile of v1, /device:TPU:0, one launch (start us, length us, event | category | flops | bytes accessed | tf_op | source)
XLA Modules:
  0.0 107.1 jit_solution(5731189011787389597)
XLA Ops:
  6.5 0.7 reshape_reshape.3
  7.3 0.5 collective-permute-start
  7.8 2.6 %collective-permute-start.1 = (bf16[1,1,4,144]{3,0,2,1:T(2,128)(2,1)S(1)}, bf16[1,1,4,144]{3,0,2,1:T(2,128)(2,1)S(1)}, u32[]{:S(2)}, u32[]{:S(2)}) collective-permute-start(bf16[1,1,4,144]{3,0,2,1:T(2,128)(2,1)S(1)} %get-tuple-element.186), channel_id=1, source_target_pairs={{0,16},{8,24},{16,0},{24,8},{1,17},{9,25},{17,1},{25,9},{2,18},{10... | collective-permute-start | bytes 3464 | tf_op jit(solution)/shard_map/ppermute | solution.py:30
  10.4 1.4 %collective-permute-start.2 = (bf16[1,1,4,144]{3,0,2,1:T(2,128)(2,1)S(1)}, bf16[1,1,4,144]{3,0,2,1:T(2,128)(2,1)S(1)}, u32[]{:S(2)}, u32[]{:S(2)}) collective-permute-start(bf16[1,1,4,144]{3,0,2,1:T(2,128)(2,1)S(1)} %get-tuple-element.185), channel_id=1, source_target_pairs={{0,24},{8,0},{16,8},{24,16},{1,25},{9,1},{17,9},{25,17},{2,26},{10... | collective-permute-start | bytes 3464 | tf_op jit(solution)/shard_map/ppermute | solution.py:30
  11.8 1.3 %reshape.166 = bf16[4,4,144]{2,1,0:T(4,128)(2,1)} reshape(bf16[2,8,144]{2,1,0:T(8,128)(2,1)} %param.13) | data formatting | bytes 9216 | tf_op jit(solution)/shard_map/reshape | solution.py:110
  13.1 3.2 %all-to-all-start = ((bf16[4,4,144]{2,1,0:T(4,128)(2,1)}), bf16[4,4,144]{2,1,0:T(4,128)(2,1)S(1)}, u32[]{:S(2)}, u32[]{:S(2)}) async-start(bf16[4,4,144]{2,1,0:T(4,128)(2,1)} %reshape.166), calls=%async_computation | async-start | bytes 16384 | tf_op jit(solution)/shard_map/all_to_all | solution.py:117
  16.4 0.7 all-gather.2.cloned.1.call-update
  17.4 0.1 neg.33
  17.5 2.6 %all-to-all-done = bf16[4,4,144]{2,1,0:T(4,128)(2,1)S(1)} async-done(((bf16[4,4,144]{2,1,0:T(4,128)(2,1)}), bf16[4,4,144]{2,1,0:T(4,128)(2,1)S(1)}, u32[]{:S(2)}, u32[]{:S(2)}) %all-to-all-start) | async-done | bytes 4640 | tf_op jit(solution)/shard_map/all_to_all | solution.py:117
  20.1 3.5 %all-to-all-start.1 = ((bf16[4,4,144,128]{3,2,1,0:T(8,128)(2,1)}), bf16[4,4,144,128]{3,2,1,0:T(8,128)(2,1)S(1)}, u32[]{:S(2)}, u32[]{:S(2)}) async-start(bf16[4,4,144,128]{3,2,1,0:T(8,128)(2,1)} %bitcast.128), calls=%async_computation.1 | async-start | bytes 1179648 | tf_op jit(solution)/shard_map/all_to_all | solution.py:115
  23.6 0.9 reduce_window_sum.11
  24.5 0.2 slice_reduce_fusion
  24.7 0.1 copy.83
  24.8 0.1 reshape.175
  24.9 8.2 %all-to-all-done.1 = bf16[4,4,144,128]{3,2,1,0:T(8,128)(2,1)S(1)} async-done(((bf16[4,4,144,128]{3,2,1,0:T(8,128)(2,1)}), bf16[4,4,144,128]{3,2,1,0:T(8,128)(2,1)S(1)}, u32[]{:S(2)}, u32[]{:S(2)}) %all-to-all-start.1) | async-done | bytes 589856 | tf_op jit(solution)/shard_map/all_to_all | solution.py:115
  33.1 3.5 %all-to-all-start.2 = ((bf16[4,4,144,128]{3,2,1,0:T(8,128)(2,1)}), bf16[4,4,144,128]{3,2,1,0:T(8,128)(2,1)S(1)}, u32[]{:S(2)}, u32[]{:S(2)}) async-start(bf16[4,4,144,128]{3,2,1,0:T(8,128)(2,1)} %bitcast.9), calls=%async_computation.2 | async-start | bytes 1179648 | tf_op jit(solution)/shard_map/all_to_all | solution.py:116
  36.6 0.2 fusion.29
  36.7 0.1 copy.84
  36.8 0.8 fusion.16
  37.6 0.1 exponential_multiply_fusion
  37.8 8.3 %all-to-all-done.2 = bf16[4,4,144,128]{3,2,1,0:T(8,128)(2,1)S(1)} async-done(((bf16[4,4,144,128]{3,2,1,0:T(8,128)(2,1)}), bf16[4,4,144,128]{3,2,1,0:T(8,128)(2,1)S(1)}, u32[]{:S(2)}, u32[]{:S(2)}) %all-to-all-start.2) | async-done | bytes 589856 | tf_op jit(solution)/shard_map/all_to_all | solution.py:116
  46.1 4.2 %all-to-all-start.3 = ((bf16[4,4,144,128]{3,2,1,0:T(8,128)(2,1)}), bf16[4,4,144,128]{3,2,1,0:T(8,128)(2,1)}, u32[]{:S(2)}, u32[]{:S(2)}) async-start(bf16[4,4,144,128]{3,2,1,0:T(8,128)(2,1)} %bitcast.17), calls=%async_computation.3 | async-start | bytes 1179648 | tf_op jit(solution)/shard_map/all_to_all | solution.py:114
  50.3 0.4 fusion.17
  50.7 2.4 %convolution_bitcast_fusion = f32[9,4,128,128]{3,2,0,1:T(8,128)S(1)} fusion(bf16[4,9,64,128]{3,2,1,0:T(8,128)(2,1)S(1)} %bitcast.121, bf16[4,9,64,128]{3,2,1,0:T(8,128)(2,1)S(1)} %bitcast.118, f32[4,9,64]{2,1,0:T(8,128)S(1)} %exponential_multiply_fusion), kind=kOutput, calls=%fused_computation.19 | convolution fusion | flops 453574656 | bytes 3548160 | tf_op jit(solution)/shard_map/ncsd,ncse->ncde/dot_general | solution.py:55
  53.1 9.4 %while.21 = (s32[]{:T(128)}, f32[4,128,128]{2,1,0:T(8,128)S(1)}, f32[4,128]{1,0:T(4,128)S(1)}, f32[4]{0:T(128)S(1)}, f32[9,4,128,128]{3,2,1,0:T(8,128)}, /*index...) while((s32[]{:T(128)}, f32[4,128,128]{2,1,0:T(8,128)S(1)}, ...), condition=%wide.region_4.5_spmd.clone, body=%wide.region_3.4_spmd.clone.sunk | while | flops 330263 | bytes 1325971 | solution.py:79
  53.1 0.7 bitcast_dynamic-update-slice_fusion.4
  53.8 0.1 fusion.42
  54.0 0.1 multiply_add_fusion.2
  54.1 0.7 bitcast_dynamic-update-slice_fusion.4
  54.9 0.1 fusion.42
  55.0 0.1 multiply_add_fusion.2
  55.2 0.7 bitcast_dynamic-update-slice_fusion.4
  55.9 0.1 fusion.42
  56.0 0.1 multiply_add_fusion.2
  56.2 0.7 bitcast_dynamic-update-slice_fusion.4
  56.9 0.1 fusion.42
  57.2 0.7 bitcast_dynamic-update-slice_fusion.4
  58.0 0.1 fusion.42
  58.3 0.7 bitcast_dynamic-update-slice_fusion.4
  59.0 0.1 fusion.42
  59.3 0.7 bitcast_dynamic-update-slice_fusion.4
  60.1 0.1 fusion.42
  60.4 0.7 bitcast_dynamic-update-slice_fusion.4
  61.1 0.1 fusion.42
  61.4 0.7 bitcast_dynamic-update-slice_fusion.4
  62.2 0.1 fusion.42
  62.4 0.1 copy.87
  62.5 1.1 %copy.88 = bf16[1,4,4,144,128]{4,3,2,1,0:T(8,128)(2,1)S(1)} copy(bf16[1,4,4,144,128]{4,3,1,2,0:T(8,128)(2,1)} %bitcast.19) | data formatting | bytes 1179648 | tf_op jit(solution)/shard_map/all_to_all | solution.py:114
  63.7 1.0 fusion.27
  64.7 0.7 fusion.31
  65.5 0.1 fusion.26
  65.6 0.8 copy-done.2
  66.4 1.3 %fusion.11 = f32[4,9,64,128]{3,2,1,0:T(8,128)S(1)} fusion(bf16[4,9,64,128]{3,2,1,0:T(8,128)(2,1)S(1)} %bitcast.127, f32[4,9,64]{2,1,0:T(8,128)S(1)} %get-tuple-element.183, f32[9,4,128,128]{3,2,1,0:T(8,128)S(1)} %copy-done.2), kind=kOutput, calls=%fused_computation.21 | convolution fusion | flops 453279744 | bytes 4137984 | tf_op jit(solution)/shard_map/ncpd,ncde->ncpe/dot_general | solution.py:94
  67.7 1.3 %fusion.15 = bf16[4,9,64,128]{3,2,1,0:T(8,128)(2,1)S(1)} fusion(f32[4,9,64,128]{3,2,1,0:T(8,128)S(1)} %fusion.11, f32[4,9,64,64]{2,3,1,0:T(8,128)S(1)} %get-tuple-element.189, bf16[4,9,64,128]{3,2,1,0:T(8,128)(2,1)S(1)} %bitcast.122, f32[4,9,64]{2,1,0:T(8,128)S(1)} %get-tuple-element.182), kind=kOutput, calls=%fused_computation.25 | convolution fusion | flops 227377152 | bytes 2958336 | tf_op jit(solution)/shard_map/ncpq,ncqe->ncpe/dot_general | solution.py:97
  69.1 0.5 copy.91
  69.5 12.6 %all_to_all.63 = bf16[1,4,576,128]{3,1,0,2:T(4,128)(2,1)S(1)} all-to-all(bf16[1,4,576,128]{3,1,0,2:T(4,128)(2,1)S(1)} %copy.91), channel_id=1, replica_groups=mesh['sp'=4,'dp'=8] {'sp'}, dimensions={2} | all-to-all | bytes 1179648 | tf_op jit(solution)/shard_map/all_to_all | solution.py:121
  82.3 0.7 fusion.18
  83.0 0.2 copy.103
  83.2 1.4 %multiply_reduce_fusion = f32[4,4,144]{1,2,0:T(8,128)S(1)} fusion(bf16[1,4,4,144,128]{4,1,3,2,0:T(4,128)(2,1)S(1)} %bitcast.116, f32[4,4,144]{1,2,0:T(8,128)S(1)} %broadcast_multiply_fusion), kind=kLoop, calls=%fused_computation.28 | loop fusion | flops 1177344 | bytes 608256 | tf_op jit(solution)/shard_map/reduce_sum | solution.py:125
  84.7 0.2 copy.104
  85.0 0.8 fusion.22
  85.8 0.2 copy.96
  85.9 9.7 %all-gather.2.cloned.1.call-done = bf16[1024,2048]{1,0:T(8,128)(2,1)} async-done(((bf16[1024,256]{1,0:T(8,128)(2,1)}), bf16[1024,2048]{1,0:T(8,128)(2,1)}) %all-gather.2.cloned.1.call-update) | async-done | bytes 4194320 | tf_op jit(solution)/shard_map/all_gather | solution.py:131
  95.6 4.6 %convolution_convert_fusion = bf16[288,2048]{1,0:T(8,128)(2,1)} fusion(bf16[1024,2048]{1,0:T(8,128)(2,1)} %all-gather.2.cloned.1.call-done, bf16[36,8,8,128]{3,2,1,0:T(8,128)(2,1)S(1)} %bitcast.129), kind=kOutput, calls=%fused_computation.16 | convolution fusion | flops 1208549376 | bytes 5963776 | tf_op jit(solution)/shard_map/dot_general | solution.py:129
  (90 shorter events, 2.0 us)
Async XLA Ops:
  7.3 9.9 %collective-permute-start = (bf16[1,1,4,144]{3,0,2,1:T(2,128)(2,1)S(1)}, bf16[1,1,4,144]{3,0,2,1:T(2,128)(2,1)S(1)}, u32[]{:S(2)}, u32[]{:S(2)}) collective-permute-start(bf16[1,1,4,144]{3,0,2,1:T(2,128)(2,1)S(1)} %get-tuple-element.187), channel_id=1, source_target_pairs={{0,8},{8,16},{16,24},{24,0},{1,9},{9,17},{17,25},{25,1},{2,10},{10... | collective-permute-start | bytes 3464 | tf_op jit(solution)/shard_map/ppermute | solution.py:30
  7.8 9.5 %collective-permute-start.1 = (bf16[1,1,4,144]{3,0,2,1:T(2,128)(2,1)S(1)}, bf16[1,1,4,144]{3,0,2,1:T(2,128)(2,1)S(1)}, u32[]{:S(2)}, u32[]{:S(2)}) collective-permute-start(bf16[1,1,4,144]{3,0,2,1:T(2,128)(2,1)S(1)} %get-tuple-element.186), channel_id=1, source_target_pairs={{0,16},{8,24},{16,0},{24,8},{1,17},{9,25},{17,1},{25,9},{2,18},{10... | collective-permute-start | bytes 3464 | tf_op jit(solution)/shard_map/ppermute | solution.py:30
  10.4 7.0 %collective-permute-start.2 = (bf16[1,1,4,144]{3,0,2,1:T(2,128)(2,1)S(1)}, bf16[1,1,4,144]{3,0,2,1:T(2,128)(2,1)S(1)}, u32[]{:S(2)}, u32[]{:S(2)}) collective-permute-start(bf16[1,1,4,144]{3,0,2,1:T(2,128)(2,1)S(1)} %get-tuple-element.185), channel_id=1, source_target_pairs={{0,24},{8,0},{16,8},{24,16},{1,25},{9,1},{17,9},{25,17},{2,26},{10... | collective-permute-start | bytes 3464 | tf_op jit(solution)/shard_map/ppermute | solution.py:30
  13.1 7.0 %all-to-all-start = ((bf16[4,4,144]{2,1,0:T(4,128)(2,1)}), bf16[4,4,144]{2,1,0:T(4,128)(2,1)S(1)}, u32[]{:S(2)}, u32[]{:S(2)}) async-start(bf16[4,4,144]{2,1,0:T(4,128)(2,1)} %reshape.166), calls=%async_computation | async-start | bytes 16384 | tf_op jit(solution)/shard_map/all_to_all | solution.py:117
  16.3 79.3 %all-gather.2.cloned.1.call-start = ((), (), s32[]{:S(2)}) async-start(), calls=%async_computation.5 | async-start | bytes 4718592 | tf_op jit(solution)/shard_map/all_gather | solution.py:131
  20.1 13.0 %all-to-all-start.1 = ((bf16[4,4,144,128]{3,2,1,0:T(8,128)(2,1)}), bf16[4,4,144,128]{3,2,1,0:T(8,128)(2,1)S(1)}, u32[]{:S(2)}, u32[]{:S(2)}) async-start(bf16[4,4,144,128]{3,2,1,0:T(8,128)(2,1)} %bitcast.128), calls=%async_computation.1 | async-start | bytes 1179648 | tf_op jit(solution)/shard_map/all_to_all | solution.py:115
  33.1 13.0 %all-to-all-start.2 = ((bf16[4,4,144,128]{3,2,1,0:T(8,128)(2,1)}), bf16[4,4,144,128]{3,2,1,0:T(8,128)(2,1)S(1)}, u32[]{:S(2)}, u32[]{:S(2)}) async-start(bf16[4,4,144,128]{3,2,1,0:T(8,128)(2,1)} %bitcast.9), calls=%async_computation.2 | async-start | bytes 1179648 | tf_op jit(solution)/shard_map/all_to_all | solution.py:116
  46.1 16.5 %all-to-all-start.3 = ((bf16[4,4,144,128]{3,2,1,0:T(8,128)(2,1)}), bf16[4,4,144,128]{3,2,1,0:T(8,128)(2,1)}, u32[]{:S(2)}, u32[]{:S(2)}) async-start(bf16[4,4,144,128]{3,2,1,0:T(8,128)(2,1)} %bitcast.17), calls=%async_computation.3 | async-start | bytes 1179648 | tf_op jit(solution)/shard_map/all_to_all | solution.py:114
  50.3 2.8 %copy-start = (bf16[1,4,4,144,128]{4,3,2,1,0:T(8,128)(2,1)}, bf16[1,4,4,144,128]{4,3,2,1,0:T(8,128)(2,1)S(1)}, u32[]{:S(2)}) copy-start(bf16[1,4,4,144,128]{4,3,2,1,0:T(8,128)(2,1)S(1)} %copy.82) | copy-start | bytes 1769476
  64.7 1.7 %copy-start.2 = (f32[9,4,128,128]{3,2,1,0:T(8,128)S(1)}, f32[9,4,128,128]{3,2,1,0:T(8,128)}, u32[]{:S(2)}) copy-start(f32[9,4,128,128]{3,2,1,0:T(8,128)} %get-tuple-element.65) | copy-start | bytes 7077892
  66.4 1.3 %copy-start.1 = (bf16[1,4,4,144,128]{4,3,2,1,0:T(8,128)(2,1)S(1)}, bf16[1,4,4,144,128]{4,3,2,1,0:T(8,128)(2,1)}, u32[]{:S(2)}) copy-start(bf16[1,4,4,144,128]{4,3,2,1,0:T(8,128)(2,1)} %copy-done) | copy-start | bytes 1769476
  83.0 1.9 %copy-start.3 = (bf16[2,8,144,128]{3,2,1,0:T(8,128)(2,1)S(1)}, bf16[2,8,144,128]{3,2,1,0:T(8,128)(2,1)}, u32[]{:S(2)}) copy-start(bf16[2,8,144,128]{3,2,1,0:T(8,128)(2,1)} %param.15) | copy-start | bytes 1769476
  83.0 1.9 %copy-start.4 = (f32[8,128]{1,0:T(8,128)S(1)}, f32[8,128]{1,0:T(8,128)}, u32[]{:S(2)}) copy-start(f32[8,128]{1,0:T(8,128)} %param.16) | copy-start | bytes 12292
Sparse Core Ops, SparseCore 0:
  19.2 76.3 all-gather.1
